TPU v7x, 32 devices: a whole 2x2x4 slice. The times are simulated.
32 devices in a mesh: ep: 8 (over z, core), tp: 4 (over y, x).
Axes of the slice: x: 2, y: 2, z: 4, core: 2. Of those that a mesh axis runs over, the one named last changes fastest.
Arguments:
- tokens: bfloat16 [128, 2048], P('ep'), may hold values from -6 to 6
- norm_gain: float32 [2048], replicated, may hold values from 0.1 to 1.9
- w_query: bfloat16 [2048, 512], P('ep', 'tp'), may hold values from -0.125 to 0.125
- w_key: bfloat16 [2048, 512], P('ep', 'tp'), may hold values from -0.125 to 0.125
- w_decay: bfloat16 [2048, 512], P('ep', 'tp'), may hold values from -0.125 to 0.125
- w_value: bfloat16 [2048, 1024], P('ep', 'tp'), may hold values from -0.125 to 0.125
- w_outgate: bfloat16 [2048, 1024], P('ep', 'tp'), may hold values from -0.125 to 0.125
- decay_rate: float32 [512], P('tp'), may hold values from 0.02 to 1
- state: float32 [128, 4, 128, 256], P('ep', 'tp'), may hold values from -15 to 15
- head_gain: float32 [256], replicated, may hold values from 0.1 to 1.9
- w_output: bfloat16 [1024, 2048], P('tp'), may hold values from -0.1875 to 0.1875
- moe_gain: float32 [2048], replicated, may hold values from 0.1 to 1.9
- expert_ids: int32 [128, 2], P('ep'), may hold values from 0 to 7, all different within a row; in each aligned block of 16 rows (0 to 15, 16 to 31, ...) at most 8 rows name the same one
- group_prob: float32 [128], P('ep'), may hold values from 0.3 to 1
- inner_prob: float32 [128, 2], P('ep'), may hold values from 0.05 to 1
- w_gate: bfloat16 [8, 2048, 2048], P('ep', None, 'tp'), may hold values from -0.125 to 0.125
- w_up: bfloat16 [8, 2048, 2048], P('ep', None, 'tp'), may hold values from -0.125 to 0.125
- w_down: bfloat16 [8, 2048, 2048], P('ep', 'tp'), may hold values from -0.125 to 0.125
Outputs:
- output: bfloat16 [128, 2048], P('ep', 'tp')
Inputs may be any that keep to these rules, and one draw needn't show every extreme that they name: `expert_ids`: the 2 experts of a token differ. In the rows of one index of ep no expert is named more than 8 times, a bound that some block reaches there.
All inputs are finite; a program needn't handle non-finite values.
Results may differ from a plain program's by a relative error of at most 0.025.
Values may be sent and summed in bfloat16 or wider, within the bound.
A program may use at most 64 MiB of HBM per device.

v0:
```python
import jax
import jax.numpy as jnp
from jax import lax
from jax.sharding import PartitionSpec as P

epsilon = 1e-05


def inverse_rms(values):
    return lax.rsqrt(jnp.mean(values * values, axis=-1, keepdims=True) + epsilon)


def slot_numbers(route_ids, experts, capacity):
    flat_ids = route_ids.reshape(-1)
    onehot = (flat_ids[:, None] == jnp.arange(experts, dtype=jnp.int32)[None, :]).astype(jnp.int32)
    earlier = jnp.cumsum(onehot, axis=0) - onehot
    within = jnp.sum(earlier * onehot, axis=1)
    return (flat_ids * capacity + within).reshape(route_ids.shape)


def expert_apply(rows, weight_gate, weight_up, weight_down):
    gate = jnp.dot(rows, weight_gate, preferred_element_type=jnp.float32)
    upper = jnp.dot(rows, weight_up, preferred_element_type=jnp.float32)
    hidden = (jax.nn.silu(gate) * upper).astype(jnp.bfloat16)
    block_out = jnp.dot(hidden, weight_down, preferred_element_type=jnp.float32).astype(
        jnp.bfloat16
    )
    summed = lax.psum_scatter(
        block_out.astype(jnp.float32).astype(jnp.bfloat16), "tp", scatter_dimension=1, tiled=True
    )
    return summed


def on_device(
    tokens,
    norm_gain,
    w_query,
    w_key,
    w_decay,
    w_value,
    w_outgate,
    decay_rate,
    state,
    head_gain,
    w_output,
    moe_gain,
    expert_ids,
    group_prob,
    inner_prob,
    w_gate,
    w_up,
    w_down,
):
    wide = jnp.float32
    narrow = jnp.bfloat16
    seq_count = tokens.shape[0]
    model_width = tokens.shape[1]
    ep_count = lax.axis_size("ep")
    heads = state.shape[1]
    key_width = state.shape[2]
    value_width = state.shape[3]
    residual = tokens.astype(wide)
    normed = (residual * inverse_rms(residual) * norm_gain).astype(narrow)
    weights = (w_query, w_key, w_decay, w_value, w_outgate)
    spread = lax.all_to_all(normed, "ep", split_axis=1, concat_axis=0, tiled=True)
    projected = lax.psum_scatter(
        jnp.concatenate(
            [jnp.dot(spread, weight, preferred_element_type=wide) for weight in weights], axis=1
        ).astype(jnp.bfloat16),
        "ep",
        scatter_dimension=0,
        tiled=True,
    ).astype(jnp.float32)
    query_cols = w_query.shape[1]
    value_cols = w_value.shape[1]
    query = projected[:, :query_cols].astype(narrow).astype(wide).reshape(
        seq_count, heads, key_width
    ) * key_width ** (-0.5)
    key_rows = (
        projected[:, query_cols : 2 * query_cols]
        .astype(narrow)
        .astype(wide)
        .reshape(seq_count, heads, key_width)
    )
    decay_pre = projected[:, 2 * query_cols : 3 * query_cols]
    value_rows = (
        projected[:, 3 * query_cols : 3 * query_cols + value_cols].astype(narrow).astype(wide)
    )
    value_rows = value_rows.reshape(seq_count, heads, value_width)
    gate_rows = (
        projected[:, 3 * query_cols + value_cols :]
        .astype(narrow)
        .astype(wide)
        .reshape(seq_count, heads, value_width)
    )
    decay = jnp.exp(jax.nn.log_sigmoid(decay_pre) * decay_rate).reshape(seq_count, heads, key_width)
    updated = decay[..., None] * state + key_rows[..., None] * value_rows[:, :, None, :]
    readout = jnp.einsum("shk,shkv->shv", query, updated, precision=lax.Precision.HIGHEST)
    gated = (readout * inverse_rms(readout) * head_gain * jax.nn.silu(gate_rows)).astype(narrow)
    head_part = jnp.dot(
        gated.reshape(seq_count, heads * value_width), w_output, preferred_element_type=wide
    )
    attention = lax.psum(head_part.astype(narrow).astype(wide).astype(jnp.bfloat16), "tp").astype(
        jnp.float32
    )
    mixed_wide = (residual + attention).astype(narrow).astype(wide)
    moe_in = (mixed_wide * inverse_rms(mixed_wide) * moe_gain).astype(narrow)
    route_weight = group_prob[:, None] * inner_prob / jnp.sum(inner_prob, axis=1, keepdims=True)
    top = expert_ids.shape[1]
    capacity = 2 * seq_count * top // ep_count
    slot_total = ep_count * capacity
    col_width = model_width // lax.axis_size("tp")
    col_start = lax.axis_index("tp") * col_width
    slots = slot_numbers(expert_ids, ep_count, capacity)
    slot_range = jnp.arange(slot_total, dtype=jnp.int32)
    combine = jnp.sum(
        jnp.where(slots[:, :, None] == slot_range[None, None, :], route_weight[:, :, None], 0.0),
        axis=1,
    )
    dispatch = jnp.any(slots[None, :, :] == slot_range[:, None, None], axis=2).astype(narrow)
    sending = jnp.dot(dispatch, moe_in, preferred_element_type=wide).astype(narrow)
    arrived = lax.all_to_all(sending, "ep", split_axis=0, concat_axis=0, tiled=True)
    expert_out = expert_apply(arrived, w_gate[0], w_up[0], w_down[0])
    returned = lax.all_to_all(expert_out, "ep", split_axis=0, concat_axis=0, tiled=True).astype(
        wide
    )
    moe_sum = jnp.dot(combine, returned, precision=lax.Precision.HIGHEST)
    own_cols = lax.dynamic_slice_in_dim(mixed_wide, col_start, col_width, 1)
    return (own_cols + moe_sum).astype(narrow)


def solution(mesh):
    placed = (
        P("ep", None),
        P(),
        P("ep", "tp"),
        P("ep", "tp"),
        P("ep", "tp"),
        P("ep", "tp"),
        P("ep", "tp"),
        P("tp"),
        P("ep", "tp", None, None),
        P(),
        P("tp", None),
        P(),
        P("ep", None),
        P("ep"),
        P("ep", None),
        P("ep", None, "tp"),
        P("ep", None, "tp"),
        P("ep", "tp", None),
    )
    return jax.shard_map(
        on_device, mesh=mesh, in_specs=placed, out_specs=P("ep", "tp"), check_vma=False
    )
```

profile of v0, /device:TPU:0, one launch (start us, length us, event | category | flops | bytes accessed | tf_op | source)
XLA Modules:
  0.0 166.4 jit_solution(632470645362486646)
XLA Ops:
  6.5 0.0 copy-start
  6.5 0.0 copy-start.5
  6.5 1.1 fusion.28
  7.7 0.9 fusion.30
  8.6 0.0 copy-start.1
  8.6 0.0 copy-start.7
  8.6 0.6 copy.56
  9.2 6.4 %all-to-all-start = ((bf16[16,8,256]{2,0,1:T(8,128)(2,1)}), bf16[16,8,256]{2,0,1:T(8,128)(2,1)S(1)}, u32[]{:S(2)}, u32[]{:S(2)}) async-start(bf16[16,8,256]{2,0,1:T(8,128)(2,1)} %bitcast.65), calls=%async_computation | async-start | bytes 131072 | tf_op jit(solution)/shard_map/all_to_all | solution.py:65
  15.6 0.0 reduce-scatter.3.cloned.1.call-start
  15.6 0.8 copy.47
  16.4 0.1 eq.20
  16.5 5.0 %all-to-all-done = bf16[16,8,256]{2,0,1:T(8,128)(2,1)S(1)} async-done(((bf16[16,8,256]{2,0,1:T(8,128)(2,1)}), bf16[16,8,256]{2,0,1:T(8,128)(2,1)S(1)}, u32[]{:S(2)}, u32[]{:S(2)}) %all-to-all-start) | async-done | bytes 65568 | tf_op jit(solution)/shard_map/all_to_all | solution.py:65
  21.5 1.1 convolution_convert_fusion.7
  22.6 0.1 copy.44
  22.7 1.1 convolution_convert_fusion.6
  23.8 0.1 copy.45
  23.9 1.1 convolution_convert_fusion.5
  25.0 0.1 copy.46
  25.1 0.0 copy-start.2
  25.1 1.1 fusion.18
  26.2 0.0 copy-start.4
  26.2 1.1 fusion.17
  27.3 0.0 copy-start.3
  27.3 0.7 copy-done.3
  28.0 0.0 reduce-scatter.3.cloned.1.call-update
  28.0 0.0 all-reduce.2.cloned.1.call-start
  28.1 0.1 fusion.48
  28.1 0.1 reduce_window_sum.11
  28.2 0.2 select_reduce_fusion.1
  28.4 0.1 reduce_sum.59
  28.5 0.1 copy.48
  28.6 0.0 copy-done.5
  28.6 28.9 %reduce-scatter.3.cloned.1.call-done = bf16[16,896]{1,0:T(8,128)(2,1)} async-done(((bf16[128,896]{1,0:T(8,128)(2,1)}), bf16[16,896]{1,0:T(8,128)(2,1)}) %reduce-scatter.3.cloned.1.call-update) | async-done | bytes 28688 | tf_op jit(solution)/shard_map/reduce_scatter | solution.py:66
  57.4 0.7 slice_convert_fusion
  58.1 0.7 slice_convert_fusion.1
  58.8 0.0 copy-done.8
  58.8 0.7 fusion.54
  59.5 3.0 %fusion.6 = f32[16,1,256]{2,1,0:T(1,128)S(1)} fusion(f32[16,128,1]{1,2,0:T(1,128)S(1)} %bitcast.73, f32[16,1,128,256]{3,2,1,0:T(8,128)} %param.26, f32[16,256]{1,0:T(8,128)S(1)} %slice_convert_fusion, f32[16,128]{1,0:T(8,128)S(1)} %slice_convert_fusion.1, f32[16,128]{1,0:T(8,128)S(1)} %get-tuple-element.7), kind=kOutput, calls=%fused_computation.9 | convolution fusion | flops 7864320 | bytes 2154496 | tf_op jit(solution)/shard_map/shk,shkv->shv/dot_general | solution.py:98
  62.6 0.1 fusion.46
  62.7 0.0 copy-done.1
  62.7 0.0 copy-done.7
  62.7 1.6 convolution_convert_fusion.2
  64.3 0.0 all-reduce.2.cloned.1.call-update
  64.4 0.0 reduce-scatter.5.cloned.1.call-start
  64.4 0.1 fusion.50
  64.5 40.1 %all-reduce.2.cloned.1.call-done = bf16[16,2048]{1,0:T(8,128)(2,1)} async-done(((bf16[16,2048]{1,0:T(8,128)(2,1)}), bf16[16,2048]{1,0:T(8,128)(2,1)}) %all-reduce.2.cloned.1.call-update) | async-done | bytes 65552 | tf_op jit(solution)/shard_map/psum | solution.py:103
  104.6 0.0 copy-done.2
  104.6 1.0 fusion.37
  105.5 0.0 copy-done.4
  105.6 1.1 fusion
  106.7 14.1 %all_to_all.43 = bf16[8,8,2048]{2,1,0:T(8,128)(2,1)S(1)} all-to-all(bf16[8,8,2048]{2,1,0:T(8,128)(2,1)S(1)} %fusion), channel_id=1, replica_groups=mesh['ep'=8,'tp'=4] {'ep'}, dimensions={0} | all-to-all | bytes 524288 | tf_op jit(solution)/shard_map/all_to_all | solution.py:122
  120.8 2.1 %fusion.4 = f32[64,512]{1,0:T(8,128)S(1)} fusion(bf16[1,2048,512]{2,1,0:T(8,128)(2,1)} %param.33, bf16[8,8,2048]{2,1,0:T(8,128)(2,1)S(1)} %all_to_all.43), kind=kOutput, calls=%fused_computation.7 | convolution fusion | flops 134217728 | bytes 2490368 | tf_op jit(solution)/shard_map/dot_general | solution.py:22
  122.9 0.0 copy-done
  122.9 0.0 copy-start.6
  122.9 0.0 copy-start.9
  122.9 3.2 %convolution_convert_fusion = bf16[64,2048]{1,0:T(8,128)(2,1)} fusion(bf16[1,512,2048]{2,1,0:T(8,128)(2,1)S(1)} %copy-done, bf16[1,2048,512]{2,1,0:T(8,128)(2,1)} %param.34, bf16[8,8,2048]{2,1,0:T(8,128)(2,1)S(1)} %all_to_all.43, f32[64,512]{1,0:T(8,128)S(1)} %fusion.4), kind=kOutput, calls=%fused_computation | convolution fusion | flops 268763136 | bytes 4849664 | tf_op jit(solution)/shard_map/dot_general | solution.py:25
  126.1 0.0 reduce-scatter.5.cloned.1.call-update
  126.1 0.0 copy-done.6
  126.2 0.0 copy-done.9
  126.2 22.4 %reduce-scatter.5.cloned.1.call-done = bf16[64,512]{1,0:T(8,128)(2,1)} async-done(((bf16[64,2048]{1,0:T(8,128)(2,1)}), bf16[64,512]{1,0:T(8,128)(2,1)}) %reduce-scatter.5.cloned.1.call-update) | async-done | bytes 65552 | tf_op jit(solution)/shard_map/reduce_scatter | solution.py:28
  148.6 4.6 %all-to-all-start.2 = ((bf16[8,8,512]{2,1,0:T(8,128)(2,1)}), bf16[8,8,512]{2,1,0:T(8,128)(2,1)S(1)}, u32[]{:S(2)}, u32[]{:S(2)}) async-start(bf16[8,8,512]{2,1,0:T(8,128)(2,1)} %bitcast.72), calls=%async_computation.4 | async-start | bytes 131072 | tf_op jit(solution)/shard_map/all_to_all | solution.py:124
  153.2 0.1 select_reduce_fusion
  153.2 5.8 %all-to-all-done.2 = bf16[8,8,512]{2,1,0:T(8,128)(2,1)S(1)} async-done(((bf16[8,8,512]{2,1,0:T(8,128)(2,1)}), bf16[8,8,512]{2,1,0:T(8,128)(2,1)S(1)}, u32[]{:S(2)}, u32[]{:S(2)}) %all-to-all-start.2) | async-done | bytes 65568 | tf_op jit(solution)/shard_map/all_to_all | solution.py:124
  159.1 0.8 fusion.21
  (10 shorter events, 0.1 us)
Async XLA Ops:
  6.5 116.3 %copy-start = (bf16[1,512,2048]{2,1,0:T(8,128)(2,1)S(1)}, bf16[1,512,2048]{2,1,0:T(8,128)(2,1)}, u32[]{:S(2)}) copy-start(bf16[1,512,2048]{2,1,0:T(8,128)(2,1)} %param.35) | copy-start | bytes 6291460
  6.5 22.0 %copy-start.5 = (s32[16,2]{0,1:T(2,128)S(1)}, s32[16,2]{0,1:T(2,128)}, u32[]{:S(2)}) copy-start(s32[16,2]{0,1:T(2,128)} %param.30) | copy-start | bytes 388
  6.5 52.3 %copy-start.8 = (f32[128]{0:T(128)S(1)}, f32[128]{0:T(128)}, u32[]{:S(2)}) copy-start(f32[128]{0:T(128)} %param.25) | copy-start | bytes 1540
  8.6 54.1 %copy-start.1 = (bf16[256,2048]{1,0:T(8,128)(2,1)S(1)}, bf16[256,2048]{1,0:T(8,128)(2,1)}, u32[]{:S(2)}) copy-start(bf16[256,2048]{1,0:T(8,128)(2,1)} %param.28) | copy-start | bytes 3145732
  8.6 54.1 %copy-start.7 = (f32[256]{0:T(256)S(1)}, f32[256]{0:T(256)}, u32[]{:S(2)}) copy-start(f32[256]{0:T(256)} %param.27) | copy-start | bytes 3076
  9.2 12.3 %all-to-all-start = ((bf16[16,8,256]{2,0,1:T(8,128)(2,1)}), bf16[16,8,256]{2,0,1:T(8,128)(2,1)S(1)}, u32[]{:S(2)}, u32[]{:S(2)}) async-start(bf16[16,8,256]{2,0,1:T(8,128)(2,1)} %bitcast.65), calls=%async_computation | async-start | bytes 131072 | tf_op jit(solution)/shard_map/all_to_all | solution.py:65
  15.6 41.8 %reduce-scatter.3.cloned.1.call-start = ((), (), s32[]{:S(2)}) async-start(), calls=%async_computation.5 | async-start | bytes 258048 | tf_op jit(solution)/shard_map/reduce_scatter | solution.py:66
  25.1 79.4 %copy-start.2 = (bf16[16,2048]{1,0:T(8,128)(2,1)S(1)}, bf16[16,2048]{1,0:T(8,128)(2,1)}, u32[]{:S(2)}) copy-start(bf16[16,2048]{1,0:T(8,128)(2,1)} %param.18) | copy-start | bytes 196612
  26.2 79.3 %copy-start.4 = (f32[2048]{0:T(1024)S(1)}, f32[2048]{0:T(1024)}, u32[]{:S(2)}) copy-start(f32[2048]{0:T(1024)} %param.29) | copy-start | bytes 24580
  27.3 0.7 copy-start.3
  28.0 76.5 %all-reduce.2.cloned.1.call-start = ((), (), s32[]{:S(2)}) async-start(), calls=%async_computation.6 | async-start | bytes 131072 | tf_op jit(solution)/shard_map/psum | solution.py:103
  64.4 84.2 %reduce-scatter.5.cloned.1.call-start = ((), (), s32[]{:S(2)}) async-start(), calls=%async_computation.7 | async-start | bytes 327680 | tf_op jit(solution)/shard_map/reduce_scatter | solution.py:28
  122.9 3.3 %copy-start.6 = (f32[16,2]{0,1:T(2,128)S(1)}, f32[16,2]{0,1:T(2,128)}, u32[]{:S(2)}) copy-start(f32[16,2]{0,1:T(2,128)} %param.32) | copy-start | bytes 388
  122.9 3.3 %copy-start.9 = (f32[16]{0:T(128)S(1)}, f32[16]{0:T(128)}, u32[]{:S(2)}) copy-start(f32[16]{0:T(128)} %param.31) | copy-start | bytes 196
  148.6 10.5 %all-to-all-start.2 = ((bf16[8,8,512]{2,1,0:T(8,128)(2,1)}), bf16[8,8,512]{2,1,0:T(8,128)(2,1)S(1)}, u32[]{:S(2)}, u32[]{:S(2)}) async-start(bf16[8,8,512]{2,1,0:T(8,128)(2,1)} %bitcast.72), calls=%async_computation.4 | async-start | bytes 131072 | tf_op jit(solution)/shard_map/all_to_all | solution.py:124
Sparse Core Ops, SparseCore 0:
  28.1 29.2 reduce-scatter.2
  64.5 40.0 all-reduce.1
  126.2 22.2 reduce-scatter.4
where the time goes:
time: 167 us; the launch traced here: 166 us
  waiting for transfers between devices  102 us (61%)
  matrix products  17.1 us (10%)
  blocking collectives  14.1 us (8%)
  between operations  13.3 us (8%)
  starting transfers between devices  11.1 us (7%)
  other arithmetic  5.74 us (3%)
  local copies, waits for them, and re-layouts  2.73 us (2%)
    psum x1, waiting for transfers between devices, on_device(): lax.psum(head_part.astype(narrow).astype(wide).astype(jnp.bfloat16), 'tp')  40.1 us
    reduce_scatter x1, waiting for transfers between devices, on_device(): lax.psum_scatter(jnp.concatenate([jnp.dot(spread, weight, preferred_eleme...  28.9 us
    reduce_scatter x1, waiting for transfers between devices, expert_apply(): lax.psum_scatter(block_out.astype(jnp.float32).astype(jnp.bfloat16), 'tp'...  22.4 us
    all_to_all x1, blocking collectives, on_device(): lax.all_to_all(sending, 'ep', split_axis=0, concat_axis=0, tiled=True)  14.1 us
    all_to_all x1, starting transfers between devices, on_device(): lax.all_to_all(normed, 'ep', split_axis=1, concat_axis=0, tiled=True)  6.35 us
    all_to_all x1, waiting for transfers between devices, on_device(): lax.all_to_all(expert_out, 'ep', split_axis=0, concat_axis=0, tiled=True)  5.84 us
    dot_general x5, matrix products, on_device(): jnp.dot(spread, weight, preferred_element_type=wide)  5.33 us
    all_to_all x1, waiting for transfers between devices, on_device(): lax.all_to_all(normed, 'ep', split_axis=1, concat_axis=0, tiled=True)  5.03 us
  transfers between devices with their start and end apart: 5, of which 5 were waited for; matrix products, arithmetic and copies ran while one was open for 1% of the time, Pallas kernels for 0%

commit v1 on v0

v1 whole, which is shorter than its diff:
```python
import functools

import jax
import jax.numpy as jnp
from jax import lax
from jax.experimental import pallas as pl
from jax.experimental.pallas import tpu as pltpu
from jax.sharding import PartitionSpec as P

epsilon = 1e-05
MESH = pl.DeviceIdType.MESH
WIDE = jnp.float32
NARROW = jnp.bfloat16


def inverse_rms(values):
    return lax.rsqrt(jnp.mean(values * values, axis=-1, keepdims=True) + epsilon)


def silu(values):
    return values / (1.0 + jnp.exp(-values))


def column(row):
    count = row.shape[1]
    shape = (count, count)
    diagonal = lax.broadcasted_iota(jnp.int32, shape, 0) == lax.broadcasted_iota(jnp.int32, shape, 1)
    return jnp.sum(jnp.where(diagonal, jnp.broadcast_to(row, shape), 0.0), axis=1, keepdims=True)


def layer(
    ep,
    tp,
    capacity,
    tokens_in, norm_gain_in, w_query_in, w_key_in, w_decay_in, w_value_in, w_outgate_in,
    decay_rate_in, state_in, head_gain_in, w_output_in, moe_gain_in, ids_in, group_in, inner_in,
    w_gate_in, w_up_in, w_down_in,
    out_ref,
    tokens, norm_gain, w_project, decay_rate, state, head_gain, w_output, moe_gain, ids, group,
    inner, w_gate, w_up, w_down,
    send1, recv1, send2, recv2, readout_rows, send3, recv3, mixed_rows, pack, send4, recv4, send6,
    recv6, pack_out, send7, recv7,
    local_sems, s1, r1, s2, r2, s3, r3, s4, r4, s6, r6, s7, r7,
):
    me_ep = lax.axis_index("ep")
    me_tp = lax.axis_index("tp")
    ahead_ep = [lax.rem(me_ep + o, ep) for o in range(ep)]
    behind_ep = [lax.rem(me_ep + ep - o, ep) for o in range(ep)]
    ahead_tp = [lax.rem(me_tp + o, tp) for o in range(tp)]

    query_cols = w_query_in.shape[1]
    value_cols = w_value_in.shape[1]
    edges = [0, query_cols, 2 * query_cols, 3 * query_cols, 3 * query_cols + value_cols,
             3 * query_cols + 2 * value_cols]
    loads = [
        (tokens_in, tokens),
        (norm_gain_in, norm_gain),
        (w_query_in, w_project.at[:, edges[0]:edges[1]]),
        (w_key_in, w_project.at[:, edges[1]:edges[2]]),
        (w_decay_in, w_project.at[:, edges[2]:edges[3]]),
        (w_value_in, w_project.at[:, edges[3]:edges[4]]),
        (w_outgate_in, w_project.at[:, edges[4]:edges[5]]),
        (decay_rate_in, decay_rate),
        (state_in, state),
        (head_gain_in, head_gain),
        (w_output_in, w_output),
        (moe_gain_in, moe_gain),
        (ids_in, ids),
        (group_in, group),
        (inner_in, inner),
        (w_gate_in.at[0], w_gate),
        (w_up_in.at[0], w_up),
        (w_down_in.at[0], w_down),
    ]
    loads = [
        pltpu.make_async_copy(source, target, local_sems.at[i])
        for i, (source, target) in enumerate(loads)
    ]
    for load in loads[:2]:
        load.start()

    barrier = pltpu.get_barrier_semaphore()
    for o in range(1, ep):
        pl.semaphore_signal(barrier, inc=1, device_id={"ep": ahead_ep[o]}, device_id_type=MESH)
    for o in range(1, tp):
        pl.semaphore_signal(barrier, inc=1, device_id={"tp": ahead_tp[o]}, device_id_type=MESH)

    for load in loads[2:]:
        load.start()

    def remote(source, target, send_sem, recv_sem, device):
        copy = pltpu.make_async_remote_copy(
            src_ref=source, dst_ref=target, send_sem=send_sem, recv_sem=recv_sem,
            device_id=device, device_id_type=MESH,
        )
        copy.start()
        return copy

    loads[0].wait()
    loads[1].wait()
    rows = tokens.shape[0]
    width = tokens.shape[1]
    slice_width = width // ep
    residual = tokens[...].astype(WIDE)
    normed = (residual * inverse_rms(residual) * norm_gain[...]).astype(NARROW)
    for e in range(ep):
        send1[e] = normed[:, e * slice_width:(e + 1) * slice_width]
    pl.semaphore_wait(barrier, ep - 1 + tp - 1)
    pending = []
    first = [
        remote(send1.at[ahead_ep[o]], recv1.at[o], s1.at[o], r1.at[o], {"ep": ahead_ep[o]})
        for o in range(1, ep)
    ]
    pending += first
    recv1[0] = send1[me_ep]

    for i in (12, 13, 14):
        loads[i].wait()
    slots = ep * capacity
    row_of = lax.broadcasted_iota(jnp.int32, (rows, slots), 1)
    expert_of = lax.rem(me_ep + row_of // capacity, ep)
    place_of = lax.rem(row_of, capacity).astype(WIDE)
    probs = inner[...]
    scale = column(group[...]) / jnp.sum(probs, axis=1, keepdims=True)
    names = ids[...]
    hits = jnp.zeros((rows, slots), WIDE)
    weights = jnp.zeros((rows, slots), WIDE)
    for k in range(names.shape[1]):
        chosen = names[:, k:k + 1] == expert_of
        hits = jnp.where(chosen, 1.0, hits)
        weights = jnp.where(chosen, scale * probs[:, k:k + 1], weights)
    square = (rows, rows)
    earlier = jnp.where(
        lax.broadcasted_iota(jnp.int32, square, 1) < lax.broadcasted_iota(jnp.int32, square, 0),
        1.0, 0.0,
    )
    rank = jnp.dot(earlier.astype(NARROW), hits.astype(NARROW), preferred_element_type=WIDE)
    held = jnp.where(jnp.abs(rank - place_of) < 0.5, hits, 0.0)
    combine = held * weights
    select = held.astype(NARROW)

    for i in range(2, 7):
        loads[i].wait()
    for copy in first:
        copy.wait_recv()
    spread = recv1[...].reshape(ep * rows, slice_width)
    partial = jnp.dot(spread, w_project[...], preferred_element_type=WIDE)
    send2[...] = partial.astype(NARROW).reshape(ep, rows, edges[5])
    second = [
        remote(send2.at[o], recv2.at[o], s2.at[o], r2.at[o], {"ep": behind_ep[o]})
        for o in range(1, ep)
    ]
    pending += second
    for i in (7, 8, 9, 10, 11):
        loads[i].wait()
    projected = partial[0:rows]
    for copy in second:
        copy.wait_recv()
    for o in range(1, ep):
        projected = projected + recv2[o].astype(WIDE)

    heads, key_width, value_width = state.shape[1], state.shape[2], state.shape[3]
    query = projected[:, edges[0]:edges[1]].astype(NARROW).astype(WIDE) * key_width ** (-0.5)
    key_rows = projected[:, edges[1]:edges[2]].astype(NARROW).astype(WIDE)
    decay_pre = projected[:, edges[2]:edges[3]]
    value_rows = projected[:, edges[3]:edges[4]].astype(NARROW).astype(WIDE)
    gate_rows = projected[:, edges[4]:edges[5]].astype(NARROW).astype(WIDE)
    decay_log = jnp.minimum(decay_pre, 0.0) - jnp.log(1.0 + jnp.exp(-jnp.abs(decay_pre)))
    decayed = query * jnp.exp(decay_log * decay_rate[...])
    gated = []
    for h in range(heads):
        keys = slice(h * key_width, (h + 1) * key_width)
        values = slice(h * value_width, (h + 1) * value_width)
        factors = decayed[:, keys].T
        for s in range(rows):
            readout_rows[s:s + 1, :] = jnp.sum(
                factors[:, s:s + 1] * state[s, h], axis=0, keepdims=True
            )
        overlap = jnp.sum(query[:, keys] * key_rows[:, keys], axis=1, keepdims=True)
        readout = readout_rows[...] + overlap * value_rows[:, values]
        gated.append(
            (readout * inverse_rms(readout) * head_gain[...] * silu(gate_rows[:, values])).astype(NARROW)
        )
    gated = gated[0] if heads == 1 else jnp.concatenate(gated, axis=1)

    send3[...] = jnp.dot(gated, w_output[...], preferred_element_type=WIDE).astype(NARROW)
    third = [
        remote(send3, recv3.at[o], s3.at[o], r3.at[o], {"tp": ahead_tp[o]}) for o in range(1, tp)
    ]
    pending += third
    attention = send3[...].astype(WIDE)
    for copy in third:
        copy.wait_recv()
    for o in range(1, tp):
        attention = attention + recv3[o].astype(WIDE)
    mixed = (residual + attention).astype(NARROW).astype(WIDE)
    mixed_rows[...] = mixed
    moe_in = (mixed * inverse_rms(mixed) * moe_gain[...]).astype(NARROW)

    pack[...] = lax.dot_general(
        select, moe_in, (((0,), (0,)), ((), ())), preferred_element_type=WIDE
    )
    fourth = []
    for o in range(1, ep):
        send4[o] = pack[o * capacity:(o + 1) * capacity, :].astype(NARROW)
    for o in range(1, ep):
        fourth.append(
            remote(send4.at[o], recv4.at[o], s4.at[o], r4.at[o], {"ep": ahead_ep[o]})
        )
    pending += fourth
    for i in (15, 16, 17):
        loads[i].wait()
    for copy in fourth:
        copy.wait_recv()
    for o in range(1, ep):
        pack[o * capacity:(o + 1) * capacity, :] = recv4[o].astype(WIDE)
    arrived = pack[...].astype(NARROW)

    gate = jnp.dot(arrived, w_gate[...], preferred_element_type=WIDE)
    upper = jnp.dot(arrived, w_up[...], preferred_element_type=WIDE)
    hidden = (silu(gate) * upper).astype(NARROW)
    col_width = width // tp

    def block(o):
        start = pl.multiple_of(ahead_tp[o] * col_width, 128)
        return jnp.dot(
            hidden, w_down[:, pl.ds(start, col_width)], preferred_element_type=WIDE
        ).astype(NARROW)

    sixth = []
    for o in range(1, tp):
        send6[o] = block(o)
        sixth.append(remote(send6.at[o], recv6.at[o], s6.at[o], r6.at[o], {"tp": ahead_tp[o]}))
    pending += sixth
    expert_out = block(0).astype(WIDE)
    for copy in sixth:
        copy.wait_recv()
    for o in range(1, tp):
        expert_out = expert_out + recv6[o].astype(WIDE)
    pack_out[...] = expert_out.astype(NARROW).astype(WIDE)

    seventh = []
    for o in range(1, ep):
        send7[o] = pack_out[o * capacity:(o + 1) * capacity, :].astype(NARROW)
    for o in range(1, ep):
        seventh.append(
            remote(send7.at[o], recv7.at[o], s7.at[o], r7.at[o], {"ep": behind_ep[o]})
        )
    pending += seventh
    own = mixed_rows[:, pl.ds(pl.multiple_of(me_tp * col_width, 128), col_width)]
    for copy in seventh:
        copy.wait_recv()
    for o in range(1, ep):
        pack_out[o * capacity:(o + 1) * capacity, :] = recv7[o].astype(WIDE)
    moe_sum = jnp.dot(
        combine, pack_out[...], precision=lax.Precision.HIGHEST, preferred_element_type=WIDE
    )
    out_ref[...] = (own + moe_sum).astype(NARROW)
    for copy in pending:
        copy.wait_send()


def on_device(
    tokens, norm_gain, w_query, w_key, w_decay, w_value, w_outgate, decay_rate, state, head_gain,
    w_output, moe_gain, expert_ids, group_prob, inner_prob, w_gate, w_up, w_down,
):
    ep = lax.axis_size("ep")
    tp = lax.axis_size("tp")
    rows, width = tokens.shape
    top = expert_ids.shape[1]
    capacity = 2 * rows * top // ep
    slots = ep * capacity
    col_width = width // tp
    project_cols = 3 * w_query.shape[1] + 2 * w_value.shape[1]
    hidden = w_gate.shape[2]
    operands = (
        tokens, norm_gain.reshape(1, -1), w_query, w_key, w_decay, w_value, w_outgate,
        decay_rate.reshape(1, -1), state, head_gain.reshape(1, -1), w_output,
        moe_gain.reshape(1, -1), expert_ids, group_prob.reshape(1, -1), inner_prob, w_gate, w_up,
        w_down,
    )
    vmem = pltpu.VMEM
    local = [
        vmem((rows, width), NARROW),
        vmem((1, width), WIDE),
        vmem((w_query.shape[0], project_cols), NARROW),
        vmem((1, decay_rate.shape[0]), WIDE),
        vmem(state.shape, WIDE),
        vmem((1, head_gain.shape[0]), WIDE),
        vmem(w_output.shape, NARROW),
        vmem((1, width), WIDE),
        vmem(expert_ids.shape, jnp.int32),
        vmem((1, rows), WIDE),
        vmem(inner_prob.shape, WIDE),
        vmem((width, hidden), NARROW),
        vmem((width, hidden), NARROW),
        vmem((hidden, width), NARROW),
    ]
    buffers = [
        vmem((ep, rows, width // ep), NARROW),
        vmem((ep, rows, width // ep), NARROW),
        vmem((ep, rows, project_cols), NARROW),
        vmem((ep, rows, project_cols), NARROW),
        vmem((rows, state.shape[3]), WIDE),
        vmem((rows, width), NARROW),
        vmem((tp, rows, width), NARROW),
        vmem((rows, width), WIDE),
        vmem((slots, width), WIDE),
        vmem((ep, capacity, width), NARROW),
        vmem((ep, capacity, width), NARROW),
        vmem((tp, slots, col_width), NARROW),
        vmem((tp, slots, col_width), NARROW),
        vmem((slots, col_width), WIDE),
        vmem((ep, capacity, col_width), NARROW),
        vmem((ep, capacity, col_width), NARROW),
    ]
    dma = pltpu.SemaphoreType.DMA
    along_ep, along_tp = [dma((ep,))] * 2, [dma((tp,))] * 2
    semaphores = (
        [dma((len(operands),))] + along_ep + along_ep + along_tp + along_ep + along_tp + along_ep
    )
    return pl.pallas_call(
        functools.partial(layer, ep, tp, capacity),
        out_shape=jax.ShapeDtypeStruct((rows, col_width), NARROW),
        in_specs=[pl.BlockSpec(memory_space=pl.ANY)] * len(operands),
        out_specs=pl.BlockSpec(memory_space=pltpu.VMEM),
        scratch_shapes=local + buffers + semaphores,
        compiler_params=pltpu.CompilerParams(
            collective_id=0, has_side_effects=True, vmem_limit_bytes=60 * 1024 * 1024
        ),
    )(*operands)


def solution(mesh):
    placed = (
        P("ep", None),
        P(),
        P("ep", "tp"),
        P("ep", "tp"),
        P("ep", "tp"),
        P("ep", "tp"),
        P("ep", "tp"),
        P("tp"),
        P("ep", "tp", None, None),
        P(),
        P("tp", None),
        P(),
        P("ep", None),
        P("ep"),
        P("ep", None),
        P("ep", None, "tp"),
        P("ep", None, "tp"),
        P("ep", "tp", None),
    )
    return jax.shard_map(
        on_device, mesh=mesh, in_specs=placed, out_specs=P("ep", "tp"), check_vma=False
    )
```

time: 167 us -> 44.2 us (0.26)
  waiting for transfers between devices: 102 us -> 0 us
  Pallas kernels: 0 us -> 40 us
  matrix products: 17.1 us -> 0 us
  blocking collectives: 14.1 us -> 0 us
  between operations: 13.3 us -> 0.01 us
  starting transfers between devices: 11.1 us -> 0 us
  other arithmetic: 5.74 us -> 0 us
    reduce_scatter x2 -> x0, waiting for transfers between devices: 51.3 us -> none  [the longest x1 28.9 us: on_device(): lax.psum_scatter(jnp.concatenate([jnp.dot(spread, weight, preferred_eleme...]
    psum x1 -> x0, waiting for transfers between devices: 40.1 us -> none  [on_device(): lax.psum(head_part.astype(narrow).astype(wide).astype(jnp.bfloat16), 'tp')]
    pallas_call x0 -> x1, Pallas kernels: none -> 40 us  [on_device(): pl.pallas_call(functools.partial(layer, ep, tp, capacity), out_shape=jax....]
    dot_general x11 -> x0, matrix products: 17.1 us -> none  [the longest x5 5.33 us: on_device(): jnp.dot(spread, weight, preferred_element_type=wide)]
    all_to_all x1 -> x0, blocking collectives: 14.1 us -> none  [on_device(): lax.all_to_all(sending, 'ep', split_axis=0, concat_axis=0, tiled=True)]
    all_to_all x2 -> x0, starting transfers between devices: 11 us -> none  [the longest x1 6.35 us: on_device(): lax.all_to_all(normed, 'ep', split_axis=1, concat_axis=0, tiled=True)]
    all_to_all x2 -> x0, waiting for transfers between devices: 10.9 us -> none  [the longest x1 5.84 us: on_device(): lax.all_to_all(expert_out, 'ep', split_axis=0, concat_axis=0, tiled=True)]
    convert_element_type x5 -> x0, other arithmetic: 3.36 us -> none  [the longest x1 0.97 us: on_device(): mixed_wide = (residual + attention).astype(narrow).astype(wide)]
  transfers between devices with their start and end apart: 5 -> 0, of which waited for: 5 -> 0; matrix products, arithmetic and copies ran while one was open for 1% -> 0% of each run, Pallas kernels for 0% -> 0%
where the time goes in v1:
time: 44.2 us; the launch traced here: 44 us
  Pallas kernels  40 us (90%)
  local copies, waits for them, and re-layouts  4.02 us (9%)
    pallas_call x1, Pallas kernels, on_device(): pl.pallas_call(functools.partial(layer, ep, tp, capacity), out_shape=jax....  40 us
    unnamed x3, local copies, waits for them, and re-layouts  4.02 us

profile of v1, /device:TPU:0, one launch (start us, length us, event | category | flops | bytes accessed | tf_op | source)
XLA Modules:
  0.0 44.0 jit_solution(11993619089131465982)
XLA Ops:
  0.0 1.4 %copy.19.ids_in = s32[16,2]{1,0:T(8,128)} copy(s32[16,2]{0,1:T(2,128)} %param.30) | data formatting | bytes 256 | tf_op args[12]
  1.4 1.3 %copy.20.inner_in = f32[16,2]{1,0:T(8,128)} copy(f32[16,2]{0,1:T(2,128)} %param.32) | data formatting | bytes 256 | tf_op args[14]
  2.7 40.0 %shard_map.172 = bf16[16,512]{1,0:T(8,128)(2,1)} custom-call(bf16[16,2048]{1,0:T(8,128)(2,1)} %tokens_in.1, f32[1,2048]{1,0:T(1,128)} %bitcast.5, bf16[256,128]{1,0:T(8,128)(2,1)} %w_query_in.1, bf16[256,128]{1,0:T(8,128)(2,1)} %w_key_in.1, bf16[256,128]{1,0:T(8,128)(2,1)} %w_decay_in.1, bf16[256,256]{1,0:T(8,128)(2,1)} %w_value_in.1, ...), custom_call_target="tpu_custom_call" | custom-call | tf_op jit(solution)/shard_map/pallas_call | solution.py:322
  42.7 1.3 %copy.22 = bf16[16,512]{1,0:T(8,128)(2,1)} copy(bf16[16,512]{1,0:T(8,128)(2,1)} %shard_map.172) | data formatting | bytes 32768

commit v2 on v1

--- a/solution.py
+++ b/solution.py
@@ -25,7 +25,16 @@
     count = row.shape[1]
     shape = (count, count)
     diagonal = lax.broadcasted_iota(jnp.int32, shape, 0) == lax.broadcasted_iota(jnp.int32, shape, 1)
-    return jnp.sum(jnp.where(diagonal, jnp.broadcast_to(row, shape), 0.0), axis=1, keepdims=True)
+    return jnp.sum(jnp.where(diagonal, jnp.broadcast_to(row, shape), jnp.zeros(shape, row.dtype)), axis=1, keepdims=True)
+
+
+def flipped(index, bits):
+    result, weight = index, 1
+    while weight <= bits:
+        if bits & weight:
+            result = result + weight * (1 - 2 * lax.rem(index // weight, 2))
+        weight *= 2
+    return result
 
 
 def layer(
@@ -38,15 +47,16 @@
     out_ref,
     tokens, norm_gain, w_project, decay_rate, state, head_gain, w_output, moe_gain, ids, group,
     inner, w_gate, w_up, w_down,
-    send1, recv1, send2, recv2, readout_rows, send3, recv3, mixed_rows, pack, send4, recv4, send6,
-    recv6, pack_out, send7, recv7,
-    local_sems, s1, r1, s2, r2, s3, r3, s4, r4, s6, r6, s7, r7,
+    send1, recv1, send_pair, recv_pair, send2, recv2, readout_rows, send3, recv3, pack, send4, recv4, recv5, send_sum,
+    recv_sum, send_scale, recv_scale, send6, recv6, pack_out, send7, recv7,
+    local_sems, s1, r1, s2, r2, s3, r3, s4, r4, s5, r5, s_sum, r_sum, s_scale, r_scale, s6, r6, s7,
+    r7,
 ):
     me_ep = lax.axis_index("ep")
     me_tp = lax.axis_index("tp")
-    ahead_ep = [lax.rem(me_ep + o, ep) for o in range(ep)]
-    behind_ep = [lax.rem(me_ep + ep - o, ep) for o in range(ep)]
-    ahead_tp = [lax.rem(me_tp + o, tp) for o in range(tp)]
+    ahead_ep = behind_ep = [flipped(me_ep, o) for o in range(ep)]
+    ahead_tp = [flipped(me_tp, o) for o in range(tp)]
+    far_tp = list(reversed(range(1, tp)))
 
     query_cols = w_query_in.shape[1]
     value_cols = w_value_in.shape[1]
@@ -99,6 +109,7 @@
     loads[0].wait()
     loads[1].wait()
     rows = tokens.shape[0]
+    half = ep // 2
     width = tokens.shape[1]
     slice_width = width // ep
     residual = tokens[...].astype(WIDE)
@@ -108,8 +119,8 @@
     pl.semaphore_wait(barrier, ep - 1 + tp - 1)
     pending = []
     first = [
-        remote(send1.at[ahead_ep[o]], recv1.at[o], s1.at[o], r1.at[o], {"ep": ahead_ep[o]})
-        for o in range(1, ep)
+        remote(send1.at[ahead_ep[o]], recv1.at[o // 2 + o % 2 * half], s1.at[o], r1.at[o], {"ep": ahead_ep[o]})
+        for o in reversed(range(1, ep))
     ]
     pending += first
     recv1[0] = send1[me_ep]
@@ -117,19 +128,25 @@
     for i in (12, 13, 14):
         loads[i].wait()
     slots = ep * capacity
+    groups = min(ep, 8)
+    group_size = ep // groups
     row_of = lax.broadcasted_iota(jnp.int32, (rows, slots), 1)
-    expert_of = lax.rem(me_ep + row_of // capacity, ep)
+    expert_of = jnp.zeros((rows, slots), jnp.int32)
+    for o in range(ep):
+        expert_of = jnp.where(row_of // capacity == o, ahead_ep[o], expert_of)
     place_of = lax.rem(row_of, capacity).astype(WIDE)
-    probs = inner[...]
-    scale = column(group[...]) / jnp.sum(probs, axis=1, keepdims=True)
-    names = ids[...]
+    top = ids.shape[0]
+    probs = [column(inner[k:k + 1, :]) for k in range(top)]
+    scale = column(group[...]) / functools.reduce(jnp.add, probs)
+    names = [column(ids[k:k + 1, :]) for k in range(top)]
     hits = jnp.zeros((rows, slots), WIDE)
     weights = jnp.zeros((rows, slots), WIDE)
-    for k in range(names.shape[1]):
-        chosen = names[:, k:k + 1] == expert_of
+    for k in range(top):
+        chosen = names[k] == expert_of
         hits = jnp.where(chosen, 1.0, hits)
-        weights = jnp.where(chosen, scale * probs[:, k:k + 1], weights)
+        weights = jnp.where(chosen, scale * probs[k], weights)
     square = (rows, rows)
+    diagonal = lax.broadcasted_iota(jnp.int32, square, 1) == lax.broadcasted_iota(jnp.int32, square, 0)
     earlier = jnp.where(
         lax.broadcasted_iota(jnp.int32, square, 1) < lax.broadcasted_iota(jnp.int32, square, 0),
         1.0, 0.0,
@@ -144,20 +161,26 @@
     for copy in first:
         copy.wait_recv()
     spread = recv1[...].reshape(ep * rows, slice_width)
-    partial = jnp.dot(spread, w_project[...], preferred_element_type=WIDE)
-    send2[...] = partial.astype(NARROW).reshape(ep, rows, edges[5])
-    second = [
-        remote(send2.at[o], recv2.at[o], s2.at[o], r2.at[o], {"ep": behind_ep[o]})
-        for o in range(1, ep)
-    ]
+    partial = jnp.dot(spread[half * rows:], w_project[...], preferred_element_type=WIDE)
+    send_pair[...] = partial.astype(NARROW).reshape(half, rows, edges[5])
+    pair = remote(send_pair, recv_pair, s2.at[0], r2.at[0], {"ep": ahead_ep[1]})
+    pending.append(pair)
+    partial = jnp.dot(spread[:half * rows], w_project[...], preferred_element_type=WIDE)
+    pair.wait_recv()
+    second = []
+    for j in reversed(range(1, half)):
+        send2[j] = (partial[j * rows:(j + 1) * rows] + recv_pair[j].astype(WIDE)).astype(NARROW)
+        second.append(
+            remote(send2.at[j], recv2.at[j], s2.at[j], r2.at[j], {"ep": ahead_ep[2 * j]})
+        )
     pending += second
+    projected = partial[:rows] + recv_pair[0].astype(WIDE)
     for i in (7, 8, 9, 10, 11):
         loads[i].wait()
-    projected = partial[0:rows]
     for copy in second:
         copy.wait_recv()
-    for o in range(1, ep):
-        projected = projected + recv2[o].astype(WIDE)
+    for j in range(1, half):
+        projected = projected + recv2[j].astype(WIDE)
 
     heads, key_width, value_width = state.shape[1], state.shape[2], state.shape[3]
     query = projected[:, edges[0]:edges[1]].astype(NARROW).astype(WIDE) * key_width ** (-0.5)
@@ -183,52 +206,113 @@
         )
     gated = gated[0] if heads == 1 else jnp.concatenate(gated, axis=1)
 
-    send3[...] = jnp.dot(gated, w_output[...], preferred_element_type=WIDE).astype(NARROW)
+    col_width = width // tp
+
+    def columns(o):
+        return pl.ds(pl.multiple_of(ahead_tp[o] * col_width, 128), col_width)
+
+    parts = jnp.dot(gated, w_output[...], preferred_element_type=WIDE).astype(NARROW)
+    for p in range(tp):
+        send3[p] = parts[:, p * col_width:(p + 1) * col_width]
     third = [
-        remote(send3, recv3.at[o], s3.at[o], r3.at[o], {"tp": ahead_tp[o]}) for o in range(1, tp)
+        remote(send3.at[ahead_tp[o]], recv3.at[o], s3.at[o], r3.at[o], {"tp": ahead_tp[o]})
+        for o in far_tp
     ]
     pending += third
-    attention = send3[...].astype(WIDE)
+    attention = send3[me_tp].astype(WIDE)
     for copy in third:
         copy.wait_recv()
     for o in range(1, tp):
         attention = attention + recv3[o].astype(WIDE)
-    mixed = (residual + attention).astype(NARROW).astype(WIDE)
-    mixed_rows[...] = mixed
-    moe_in = (mixed * inverse_rms(mixed) * moe_gain[...]).astype(NARROW)
-
+    mixed = (tokens[:, columns(0)].astype(WIDE) + attention).astype(NARROW).astype(WIDE)
+
+    gained = (mixed * moe_gain[:, columns(0)]).astype(NARROW)
     pack[...] = lax.dot_general(
-        select, moe_in, (((0,), (0,)), ((), ())), preferred_element_type=WIDE
-    )
-    fourth = []
-    for o in range(1, ep):
-        send4[o] = pack[o * capacity:(o + 1) * capacity, :].astype(NARROW)
-    for o in range(1, ep):
-        fourth.append(
-            remote(send4.at[o], recv4.at[o], s4.at[o], r4.at[o], {"ep": ahead_ep[o]})
-        )
+        select, gained, (((0,), (0,)), ((), ())), preferred_element_type=WIDE
+    )
+    for o in range(ep):
+        target = send4 if o else recv4
+        target[o] = pack[o * capacity:(o + 1) * capacity, :].astype(NARROW)
+    fourth = [
+        remote(send4.at[o], recv4.at[o], s4.at[o], r4.at[o], {"ep": ahead_ep[o]})
+        for o in reversed(range(1, ep))
+    ]
     pending += fourth
+
+    squares = jnp.sum(mixed * mixed, axis=1, keepdims=True)
+    send_sum[...] = jnp.sum(jnp.where(diagonal, squares, 0.0), axis=0, keepdims=True)
+    sums = [
+        remote(send_sum, recv_sum.at[o], s_sum.at[o], r_sum.at[o], {"tp": ahead_tp[o]})
+        for o in range(1, tp)
+    ]
+    pending += sums
+
+    fifth = []
+
+    def forward(g):
+        for o in far_tp:
+            fifth.append(
+                remote(
+                    recv4.at[pl.ds(g * group_size, group_size)],
+                    recv5.at[o, pl.ds(g * group_size, group_size)],
+                    s5.at[o, g], r5.at[o, g], {"tp": ahead_tp[o]},
+                )
+            )
+
+    if group_size == 1:
+        forward(0)
+    for copy in sums:
+        copy.wait_recv()
+    total = send_sum[...]
+    for o in range(1, tp):
+        total = total + recv_sum[o]
+    scales = column(lax.rsqrt(total / width + epsilon))
+    send_scale[...] = jnp.sum(held * scales, axis=0, keepdims=True)
+    scaled = [
+        remote(send_scale, recv_scale.at[o], s_scale.at[o], r_scale.at[o], {"ep": ahead_ep[o]})
+        for o in reversed(range(1, ep))
+    ]
+    pending += scaled
+    for g in range(1 if group_size == 1 else 0, groups):
+        for o in range(max(1, g * group_size), (g + 1) * group_size):
+            fourth[ep - 1 - o].wait_recv()
+        forward(g)
+    pending += fifth
     for i in (15, 16, 17):
         loads[i].wait()
-    for copy in fourth:
-        copy.wait_recv()
+
+    gate = jnp.zeros((slots, w_gate.shape[1]), WIDE)
+    upper = gate
+    for o in range(tp):
+        if o:
+            for g in range(groups):
+                fifth[g * (tp - 1) + tp - 1 - o].wait_recv()
+        for e in range(ep):
+            pack[e * capacity:(e + 1) * capacity, :] = (recv5[o, e] if o else recv4[e]).astype(WIDE)
+        arrived = pack[...].astype(NARROW)
+        depth = pl.ds(
+            pl.multiple_of(ahead_tp[o] * col_width, 128), col_width
+        )
+        gate = gate + jnp.dot(arrived, w_gate[depth, :], preferred_element_type=WIDE)
+        upper = upper + jnp.dot(arrived, w_up[depth, :], preferred_element_type=WIDE)
+    for copy in scaled:
+        copy.wait_recv()
+    slot_of = lax.broadcasted_iota(jnp.int32, (1, slots), 1) // capacity
+    slot_scale = jnp.where(slot_of == 0, send_scale[...], 0.0)
     for o in range(1, ep):
-        pack[o * capacity:(o + 1) * capacity, :] = recv4[o].astype(WIDE)
-    arrived = pack[...].astype(NARROW)
-
-    gate = jnp.dot(arrived, w_gate[...], preferred_element_type=WIDE)
-    upper = jnp.dot(arrived, w_up[...], preferred_element_type=WIDE)
+        slot_scale = jnp.where(slot_of == o, recv_scale[o], slot_scale)
+    slot_scale = column(slot_scale)
+    gate = gate * slot_scale
+    upper = upper * slot_scale
     hidden = (silu(gate) * upper).astype(NARROW)
-    col_width = width // tp
 
     def block(o):
-        start = pl.multiple_of(ahead_tp[o] * col_width, 128)
         return jnp.dot(
-            hidden, w_down[:, pl.ds(start, col_width)], preferred_element_type=WIDE
+            hidden, w_down[:, columns(o)], preferred_element_type=WIDE
         ).astype(NARROW)
 
     sixth = []
-    for o in range(1, tp):
+    for o in far_tp:
         send6[o] = block(o)
         sixth.append(remote(send6.at[o], recv6.at[o], s6.at[o], r6.at[o], {"tp": ahead_tp[o]}))
     pending += sixth
@@ -242,12 +326,11 @@
     seventh = []
     for o in range(1, ep):
         send7[o] = pack_out[o * capacity:(o + 1) * capacity, :].astype(NARROW)
-    for o in range(1, ep):
+    for o in reversed(range(1, ep)):
         seventh.append(
             remote(send7.at[o], recv7.at[o], s7.at[o], r7.at[o], {"ep": behind_ep[o]})
         )
     pending += seventh
-    own = mixed_rows[:, pl.ds(pl.multiple_of(me_tp * col_width, 128), col_width)]
     for copy in seventh:
         copy.wait_recv()
     for o in range(1, ep):
@@ -255,7 +338,7 @@
     moe_sum = jnp.dot(
         combine, pack_out[...], precision=lax.Precision.HIGHEST, preferred_element_type=WIDE
     )
-    out_ref[...] = (own + moe_sum).astype(NARROW)
+    out_ref[...] = (mixed + moe_sum).astype(NARROW)
     for copy in pending:
         copy.wait_send()
 
@@ -276,7 +359,7 @@
     operands = (
         tokens, norm_gain.reshape(1, -1), w_query, w_key, w_decay, w_value, w_outgate,
         decay_rate.reshape(1, -1), state, head_gain.reshape(1, -1), w_output,
-        moe_gain.reshape(1, -1), expert_ids, group_prob.reshape(1, -1), inner_prob, w_gate, w_up,
+        moe_gain.reshape(1, -1), expert_ids.T, group_prob.reshape(1, -1), inner_prob.T, w_gate, w_up,
         w_down,
     )
     vmem = pltpu.VMEM
@@ -289,9 +372,9 @@
         vmem((1, head_gain.shape[0]), WIDE),
         vmem(w_output.shape, NARROW),
         vmem((1, width), WIDE),
-        vmem(expert_ids.shape, jnp.int32),
+        vmem((top, rows), jnp.int32),
         vmem((1, rows), WIDE),
-        vmem(inner_prob.shape, WIDE),
+        vmem((top, rows), WIDE),
         vmem((width, hidden), NARROW),
         vmem((width, hidden), NARROW),
         vmem((hidden, width), NARROW),
@@ -299,15 +382,21 @@
     buffers = [
         vmem((ep, rows, width // ep), NARROW),
         vmem((ep, rows, width // ep), NARROW),
-        vmem((ep, rows, project_cols), NARROW),
-        vmem((ep, rows, project_cols), NARROW),
+        vmem((ep // 2, rows, project_cols), NARROW),
+        vmem((ep // 2, rows, project_cols), NARROW),
+        vmem((ep // 2, rows, project_cols), NARROW),
+        vmem((ep // 2, rows, project_cols), NARROW),
         vmem((rows, state.shape[3]), WIDE),
-        vmem((rows, width), NARROW),
-        vmem((tp, rows, width), NARROW),
-        vmem((rows, width), WIDE),
-        vmem((slots, width), WIDE),
-        vmem((ep, capacity, width), NARROW),
-        vmem((ep, capacity, width), NARROW),
+        vmem((tp, rows, col_width), NARROW),
+        vmem((tp, rows, col_width), NARROW),
+        vmem((slots, col_width), WIDE),
+        vmem((ep, capacity, col_width), NARROW),
+        vmem((ep, capacity, col_width), NARROW),
+        vmem((tp, ep, capacity, col_width), NARROW),
+        vmem((1, rows), WIDE),
+        vmem((tp, 1, rows), WIDE),
+        vmem((1, slots), WIDE),
+        vmem((ep, 1, slots), WIDE),
         vmem((tp, slots, col_width), NARROW),
         vmem((tp, slots, col_width), NARROW),
         vmem((slots, col_width), WIDE),
@@ -317,7 +406,8 @@
     dma = pltpu.SemaphoreType.DMA
     along_ep, along_tp = [dma((ep,))] * 2, [dma((tp,))] * 2
     semaphores = (
-        [dma((len(operands),))] + along_ep + along_ep + along_tp + along_ep + along_tp + along_ep
+        [dma((len(operands),))] + along_ep + along_ep + along_tp + along_ep
+        + [dma((tp, min(ep, 8)))] * 2 + along_tp + along_ep + along_tp + along_ep
     )
     return pl.pallas_call(
         functools.partial(layer, ep, tp, capacity),

time: 44.2 us -> 39.6 us (0.90)
  local copies, waits for them, and re-layouts: 4.02 us -> 1.32 us
  Pallas kernels: 40 us -> 38 us
    unnamed x3 -> x1, local copies, waits for them, and re-layouts: 4.02 us -> 1.32 us
    pallas_call x1, Pallas kernels: 40 us -> 38 us  [on_device(): pl.pallas_call(functools.partial(layer, ep, tp, capacity), out_shape=jax....]
where the time goes in v2:
time: 39.6 us; the launch traced here: 39.4 us
  Pallas kernels  38 us (96%)
  local copies, waits for them, and re-layouts  1.32 us (3%)
    pallas_call x1, Pallas kernels, on_device(): pl.pallas_call(functools.partial(layer, ep, tp, capacity), out_shape=jax....  38 us
    unnamed x1, local copies, waits for them, and re-layouts  1.32 us

profile of v2, /device:TPU:0, one launch (start us, length us, event | category | flops | bytes accessed | tf_op | source)
XLA Modules:
  0.0 39.4 jit_solution(9517541451112402761)
XLA Ops:
  0.0 38.0 %shard_map.172 = bf16[16,512]{1,0:T(8,128)(2,1)} custom-call(bf16[16,2048]{1,0:T(8,128)(2,1)} %tokens_in.1, f32[1,2048]{1,0:T(1,128)} %bitcast.7, bf16[256,128]{1,0:T(8,128)(2,1)} %w_query_in.1, bf16[256,128]{1,0:T(8,128)(2,1)} %w_key_in.1, bf16[256,128]{1,0:T(8,128)(2,1)} %w_decay_in.1, bf16[256,256]{1,0:T(8,128)(2,1)} %w_value_in.1, ...), custom_call_target="tpu_custom_call" | custom-call | tf_op jit(solution)/shard_map/pallas_call | solution.py:412
  38.1 1.3 %copy.20 = bf16[16,512]{1,0:T(8,128)(2,1)} copy(bf16[16,512]{1,0:T(8,128)(2,1)} %shard_map.172) | data formatting | bytes 32768

commit v3 on v2

--- a/solution.py
+++ b/solution.py
@@ -259,8 +259,13 @@
                 )
             )
 
-    if group_size == 1:
-        forward(0)
+    def relay(first_group, last_group):
+        for g in range(first_group, last_group):
+            for o in range(max(1, g * group_size), (g + 1) * group_size):
+                fourth[ep - 1 - o].wait_recv()
+            forward(g)
+
+    relay(0, groups // 2)
     for copy in sums:
         copy.wait_recv()
     total = send_sum[...]
@@ -273,10 +278,7 @@
         for o in reversed(range(1, ep))
     ]
     pending += scaled
-    for g in range(1 if group_size == 1 else 0, groups):
-        for o in range(max(1, g * group_size), (g + 1) * group_size):
-            fourth[ep - 1 - o].wait_recv()
-        forward(g)
+    relay(groups // 2, groups)
     pending += fifth
     for i in (15, 16, 17):
         loads[i].wait()
@@ -411,7 +413,7 @@
     )
     return pl.pallas_call(
         functools.partial(layer, ep, tp, capacity),
-        out_shape=jax.ShapeDtypeStruct((rows, col_width), NARROW),
+        out_shape=pltpu.VMEM((rows, col_width), NARROW),
         in_specs=[pl.BlockSpec(memory_space=pl.ANY)] * len(operands),
         out_specs=pl.BlockSpec(memory_space=pltpu.VMEM),
         scratch_shapes=local + buffers + semaphores,

time: 39.6 us -> 37.9 us (0.957)
  Pallas kernels: 38 us -> 37.2 us
  local copies, waits for them, and re-layouts: 1.32 us -> 0.61 us
    pallas_call x1, Pallas kernels: 38 us -> 37.2 us  [on_device(): pl.pallas_call(functools.partial(layer, ep, tp, capacity), out_shape=pltp...]
    unnamed x1, local copies, waits for them, and re-layouts: 1.32 us -> 0.61 us
where the time goes in v3:
time: 37.9 us; the launch traced here: 37.8 us
  Pallas kernels  37.2 us (98%)
  local copies, waits for them, and re-layouts  0.61 us (2%)
    pallas_call x1, Pallas kernels, on_device(): pl.pallas_call(functools.partial(layer, ep, tp, capacity), out_shape=pltp...  37.2 us

profile of v3, /device:TPU:0, one launch (start us, length us, event | category | flops | bytes accessed | tf_op | source)
XLA Modules:
  0.0 37.8 jit_solution(9759384841247520561)
XLA Ops:
  0.0 37.2 %shard_map.172 = bf16[16,512]{1,0:T(8,128)(2,1)S(1)} custom-call(bf16[16,2048]{1,0:T(8,128)(2,1)} %tokens_in.1, f32[1,2048]{1,0:T(1,128)} %bitcast.7, bf16[256,128]{1,0:T(8,128)(2,1)} %w_query_in.1, bf16[256,128]{1,0:T(8,128)(2,1)} %w_key_in.1, bf16[256,128]{1,0:T(8,128)(2,1)} %w_decay_in.1, bf16[256,256]{1,0:T(8,128)(2,1)} %w_value_in.1, ...), custom_call_target="tpu_custom_call" | custom-call | tf_op jit(solution)/shard_map/pallas_call | solution.py:414
  37.2 0.6 %copy.20 = bf16[16,512]{1,0:T(8,128)(2,1)} copy(bf16[16,512]{1,0:T(8,128)(2,1)S(1)} %shard_map.172) | data formatting | bytes 32768
